TPU v7x, 32 devices: a whole 2x2x4 slice. The times are simulated.
32 devices in a mesh: sp: 8 (over z, y), tp: 4 (over x, core).
Axes of the slice: x: 2, y: 2, z: 4, core: 2. Of those that a mesh axis runs over, the one named last changes fastest.
Arguments:
- query_proj: bfloat16 [2048, 2048], P('sp', 'tp'), may hold values from -240 to 240
- key_projection: bfloat16 [2048, 512], P('sp', 'tp'), may hold values from -6 to 6
- value_projection: bfloat16 [2048, 512], P('sp', 'tp'), may hold values from -6 to 6
- sink_logit: float32 [32], P('tp'), may hold values from 1 to 6
- residual: bfloat16 [2048, 2048], P('sp'), may hold values from -3 to 3
- w_out: bfloat16 [2048, 2048], P('tp'), may hold values from -1 to 1
- norm_gain: float32 [2048], replicated, may hold values from 0.1 to 1.9
- routes: int32 [2048, 2], P('sp'), may hold values from 0 to 7, all different within a row; in each aligned block of 256 rows (0 to 255, 256 to 511, ...) at most 128 rows name the same one
- route_weights: float32 [2048, 2], P('sp'), may hold values from 0.1 to 1
- w_gate: bfloat16 [8, 2048, 2560], P('sp', None, 'tp'), may hold values from -0.125 to 0.125
- w_up: bfloat16 [8, 2048, 2560], P('sp', None, 'tp'), may hold values from -0.125 to 0.125
- w_down: bfloat16 [8, 2560, 2048], P('sp', 'tp'), may hold values from -0.125 to 0.125
Outputs:
- layer_out: bfloat16 [2048, 2048], P('sp', 'tp')
Inputs may be any that keep to these rules, and one draw needn't show every extreme that they name: `routes`: within the rows of one index of sp (aligned blocks of 256 tokens), no expert is named more than 128 times, and in some block one expert is named exactly 128 times. The two experts of a token differ.
All inputs are finite; a program needn't handle non-finite values.
Results may differ from a plain program's by a relative error of at most 0.015.
Values may be sent and summed in bfloat16 or wider, within the bound.
A program may use at most 64 MiB of HBM per device.

v0:
```python
import jax
import jax.numpy as jnp
from jax import lax
from jax.sharding import PartitionSpec as P

HEAD_SIZE = 64
WINDOW = 128
GRID_W = 64


ROPE_BASE = 10000.0
NORM_EPS = 1e-06


def padded(cells, sides, width):
    for axis, dim in sides:
        count = lax.axis_size(axis)
        ends = count - 1
        head = lax.slice_in_dim(cells, 0, width, axis=dim)
        tail = lax.slice_in_dim(cells, cells.shape[dim] - width, cells.shape[dim], axis=dim)
        cells = jnp.concatenate(
            [
                lax.ppermute(tail, axis, [(i, (i + 1) % count) for i in range(ends)]),
                cells,
                lax.ppermute(head, axis, [((i + 1) % count, i) for i in range(ends)]),
            ],
            axis=dim,
        )
    return cells


def rotate_pair(values_half, angles):
    first_half, second = jnp.split(values_half, 2, axis=-1)
    cosine = jnp.cos(angles)[:, None, :]
    sine_part = jnp.sin(angles)[:, None, :]
    return jnp.concatenate(
        [first_half * cosine - second * sine_part, second * cosine + first_half * sine_part],
        axis=-1,
    )


def axial_rotation(heads_in, token_positions):
    half_dim = HEAD_SIZE // 2
    inverse = ROPE_BASE ** (-jnp.arange(0, half_dim, 2, dtype=jnp.float32) / half_dim)
    row_angles = (token_positions // GRID_W).astype(jnp.float32)[:, None] * inverse
    col_angles = (token_positions % GRID_W).astype(jnp.float32)[:, None] * inverse
    as_float = heads_in.astype(jnp.float32)
    return jnp.concatenate(
        [
            rotate_pair(as_float[..., :half_dim], row_angles),
            rotate_pair(as_float[..., half_dim:], col_angles),
        ],
        axis=-1,
    )


def attend_block(query_rows, key_rows, value_rows, sink_logit, query_pos, key_pos, total_rows):
    kv_heads = key_rows.shape[1]
    groups = query_rows.shape[1] // kv_heads
    grouped = query_rows.reshape(query_rows.shape[0], kv_heads, groups, HEAD_SIZE)
    scores = jnp.einsum(
        "qkgd,jkd->kgqj", grouped, key_rows, preferred_element_type=jnp.float32
    ) * HEAD_SIZE ** (-0.5)
    in_window = (
        (jnp.abs(key_pos[None, :] - query_pos[:, None]) <= WINDOW)
        & (key_pos[None, :] >= 0)
        & (key_pos[None, :] < total_rows)
    )
    scores = jnp.where(in_window[None, None], scores, -jnp.inf)
    sink_col = sink_logit.reshape(kv_heads, groups, 1, 1)
    largest = jnp.maximum(jnp.max(scores, axis=-1, keepdims=True), sink_col)
    exp_scores = jnp.exp(scores - largest)
    denominator = jnp.sum(exp_scores, axis=-1, keepdims=True) + jnp.exp(sink_col - largest)
    weights_bf = (exp_scores / denominator).astype(jnp.bfloat16)
    mixed_heads = jnp.einsum(
        "kgqj,jkd->qkgd", weights_bf, value_rows, preferred_element_type=jnp.float32
    )
    return mixed_heads.astype(jnp.bfloat16).reshape(query_rows.shape[0], -1)


def local(
    query_proj,
    key_projection,
    value_projection,
    sink_logit,
    residual,
    w_out,
    norm_gain,
    routes,
    route_weights,
    w_gate,
    w_up,
    w_down,
):
    tok_rows = query_proj.shape[0]
    seq_devices = lax.axis_size("sp")
    total_rows = tok_rows * seq_devices
    offset = lax.axis_index("sp") * tok_rows
    kv_width = key_projection.shape[1]
    joined = jnp.concatenate([key_projection, value_projection], axis=1)
    widened = padded(joined, (("sp", 0),), WINDOW)
    query_pos = offset + jnp.arange(tok_rows, dtype=jnp.int32)
    key_pos = offset - WINDOW + jnp.arange(tok_rows + 2 * WINDOW, dtype=jnp.int32)
    rot_q = axial_rotation(query_proj.reshape(tok_rows, -1, HEAD_SIZE), query_pos).astype(
        jnp.bfloat16
    )
    rotated_keys = axial_rotation(
        widened[:, :kv_width].reshape(-1, kv_width // HEAD_SIZE, HEAD_SIZE), key_pos
    ).astype(jnp.bfloat16)
    value_head_rows = widened[:, kv_width:].reshape(-1, kv_width // HEAD_SIZE, HEAD_SIZE)
    attended = attend_block(
        rot_q, rotated_keys, value_head_rows, sink_logit, query_pos, key_pos, total_rows
    )
    partial_value = jnp.dot(attended, w_out, preferred_element_type=jnp.float32)
    width = partial_value.shape[1]
    col_blocks = lax.axis_size("tp")
    col_width = width // col_blocks
    col_start = lax.axis_index("tp") * col_width
    summed = lax.psum(partial_value.astype(jnp.bfloat16), "tp").astype(jnp.float32)
    stream = (residual.astype(jnp.float32) + summed).astype(jnp.bfloat16)
    as_float = stream.astype(jnp.float32)
    normed = (
        as_float
        * lax.rsqrt(jnp.mean(as_float * as_float, axis=-1, keepdims=True) + NORM_EPS)
        * norm_gain
    ).astype(jnp.bfloat16)
    stream_cols = lax.dynamic_slice_in_dim(stream, col_start, col_width, 1)
    top_count = routes.shape[1]
    experts = w_gate.shape[0] * seq_devices
    capacity = 2 * top_count * tok_rows // experts
    flat_routes = routes.reshape(-1)
    onehot = (flat_routes[:, None] == jnp.arange(experts, dtype=jnp.int32)[None, :]).astype(
        jnp.int32
    )
    slot_number = jnp.sum(jnp.cumsum(onehot, axis=0) * onehot, axis=1) - 1
    destination = flat_routes * capacity + slot_number
    buffer = (
        jnp.zeros((experts * capacity, width), jnp.bfloat16)
        .at[destination]
        .set(jnp.repeat(normed, top_count, axis=0))
        .reshape(experts, capacity, width)
    )
    quarter = capacity // col_blocks
    own_slots = lax.dynamic_slice_in_dim(buffer, lax.axis_index("tp") * quarter, quarter, 1)
    arrived = lax.all_to_all(own_slots, "sp", split_axis=0, concat_axis=0, tiled=True)
    joined_slots = lax.all_gather(arrived, "tp", axis=1, tiled=True)
    sources, slot_count, _ = joined_slots.shape
    expert_rows = joined_slots.reshape(-1, width)
    gate_part = jnp.dot(expert_rows, w_gate[0], preferred_element_type=jnp.float32)
    up_part = jnp.dot(expert_rows, w_up[0], preferred_element_type=jnp.float32)
    hidden = (jax.nn.silu(gate_part) * up_part).astype(jnp.bfloat16)
    partial_rows = jnp.dot(hidden, w_down[0], preferred_element_type=jnp.float32)
    col_sums = lax.psum_scatter(
        partial_rows.astype(jnp.bfloat16), "tp", scatter_dimension=1, tiled=True
    )
    returned = lax.all_to_all(
        col_sums.reshape(sources, slot_count, col_width),
        "sp",
        split_axis=0,
        concat_axis=0,
        tiled=True,
    )
    picked = (
        returned.reshape(-1, col_width)[destination]
        .astype(jnp.float32)
        .reshape(tok_rows, top_count, col_width)
    )
    mixture = jnp.sum(picked * route_weights[:, :, None], axis=1)
    return (stream_cols.astype(jnp.float32) + mixture).astype(jnp.bfloat16)


def solution(mesh):
    return jax.shard_map(
        local,
        mesh=mesh,
        in_specs=(
            P("sp", "tp"),
            P("sp", "tp"),
            P("sp", "tp"),
            P("tp"),
            P("sp", None),
            P("tp", None),
            P(),
            P("sp", None),
            P("sp", None),
            P("sp", None, "tp"),
            P("sp", None, "tp"),
            P("sp", "tp", None),
        ),
        out_specs=P("sp", "tp"),
        check_vma=False,
    )
```

profile of v0, /device:TPU:0, one launch (start us, length us, event | category | flops | bytes accessed | tf_op | source)
XLA Modules:
  0.0 277.2 jit_solution(1034085529072347477)
XLA Ops:
  6.5 1.0 constant_dynamic-update-slice_fusion.1
  9.1 5.5 %collective-permute-start = (bf16[128,256]{1,0:T(8,128)(2,1)}, bf16[128,256]{1,0:T(8,128)(2,1)}, u32[]{:S(2)}, u32[]{:S(2)}) collective-permute-start(bf16[128,256]{1,0:T(8,128)(2,1)} %get-tuple-element.21), channel_id=1, source_target_pairs={{0,4},{4,8},{8,12},{12,16},{16,20},{20,24},{24,28},{1,5},{5,9},{9,... | collective-permute-start | bytes 196616 | tf_op jit(solution)/shard_map/ppermute | solution.py:23
  14.6 1.3 collective-permute-start.1
  20.4 1.3 broadcast_multiply_fusion
  21.7 1.1 copy.23
  22.8 1.3 max.18
  24.1 1.5 multiply_cosine_fusion.1
  26.5 1.1 reduce-window.6
  27.6 0.9 fusion.19
  31.7 0.9 pad_maximum_fusion
  33.7 1.7 fusion.1
  35.5 1.8 copy-done.2
  38.4 3.5 %fusion.15 = bf16[2,64,4,256]{3,1,2,0:T(8,128)(2,1)S(1)} fusion(bf16[512,2,64,1]{0,2,3,1:T(8,128)(2,1)S(1)} %bitcast.68, f32[2,512,256,4]{2,1,3,0:T(8,128)} %copy-done.2, f32[2,4,256]{2,1,0:T(4,128)S(1)} %exponential_add_fusion, f32[2,4,256]{2,1,0:T(4,128)S(1)} %broadcast_maximum_fusion, pred[256,512]{0,1:T(8,128)(4,1)S(1)} %fusion.19), kind=kOutput, calls=%fused_computation.24 | convolution fusion | flops 139591680 | bytes 4734976 | tf_op jit(solution)/shard_map/kgqj,jkd->qkgd/dot_general | solution.py:75
  42.0 1.8 convolution_convert_fusion.1
  44.2 38.5 %all-reduce.2.cloned.1.call-done = bf16[256,2048]{1,0:T(8,128)(2,1)} async-done(((bf16[256,2048]{1,0:T(8,128)(2,1)}), bf16[256,2048]{1,0:T(8,128)(2,1)}) %all-reduce.2.cloned.1.call-update) | async-done | bytes 1048592 | tf_op jit(solution)/shard_map/psum | solution.py:119
  82.7 2.0 fusion.7
  84.7 1.0 copy-done.1
  86.0 2.6 broadcast_in_dim.15
  88.6 4.1 %reshape.478 = bf16[512,2048]{1,0:T(8,128)(2,1)} reshape(bf16[256,2,2048]{2,1,0:T(2,128)(2,1)} %broadcast_in_dim.15) | data formatting | bytes 4194304 | tf_op jit(solution)/shard_map/reshape | solution.py:140
  92.7 7.2 %scatter_custom_fusion = bf16[1024,2048]{1,0:T(8,128)(2,1)} fusion(s32[512]{0:T(512)S(1)} %bitcast.73, bf16[512,2048]{1,0:T(8,128)(2,1)} %reshape.478, bf16[]{:T(256)} %constant.97.clone.1), kind=kCustom, calls=%fused_computation.20 | custom fusion | bytes 4194816 | tf_op jit(solution)/shard_map/scatter | solution.py:140
  99.9 1.3 constant_dynamic-slice_fusion
  101.2 30.7 %all_to_all.10 = bf16[8,32,2048]{2,1,0:T(8,128)(2,1)} all-to-all(bf16[8,32,2048]{2,1,0:T(8,128)(2,1)S(1)} %constant_dynamic-slice_fusion), channel_id=1, replica_groups=mesh['sp'=8,'tp'=4] {'sp'}, dimensions={0} | all-to-all | bytes 2097152 | tf_op jit(solution)/shard_map/all_to_all | solution.py:145
  132.2 33.2 %all-gather.2.cloned.1.call-done = bf16[8,128,2048]{2,1,0:T(8,128)(2,1)} async-done(((bf16[8,32,2048]{2,1,0:T(8,128)(2,1)}), bf16[8,128,2048]{2,1,0:T(8,128)(2,1)}) %all-gather.2.cloned.1.call-update) | async-done | bytes 4194320 | tf_op jit(solution)/shard_map/all_gather | solution.py:146
  165.4 8.0 %fusion.3 = f32[1024,640]{1,0:T(8,128)} fusion(bf16[1024,2048]{1,0:T(8,128)(2,1)} %bitcast.76, bf16[1,2048,640]{2,1,0:T(8,128)(2,1)} %param.22), kind=kOutput, calls=%fused_computation.11 | convolution fusion | flops 2684354560 | bytes 9437184 | tf_op jit(solution)/shard_map/dot_general | solution.py:150
  173.4 12.1 %convolution_convert_fusion = bf16[1024,2048]{1,0:T(8,128)(2,1)} fusion(bf16[1,640,2048]{2,1,0:T(8,128)(2,1)S(1)} %copy-done, f32[1024,640]{1,0:T(8,128)} %fusion.3, bf16[1024,2048]{1,0:T(8,128)(2,1)} %bitcast.77, bf16[1,2048,640]{2,1,0:T(8,128)(2,1)} %param.21), kind=kOutput, calls=%fused_computation.5 | convolution fusion | flops 5374738432 | bytes 16252928 | tf_op jit(solution)/shard_map/dot_general | solution.py:152
  185.5 44.6 %reduce-scatter.2.cloned.1.call-done = bf16[1024,512]{1,0:T(8,128)(2,1)} async-done(((bf16[1024,2048]{1,0:T(8,128)(2,1)}), bf16[1024,512]{1,0:T(8,128)(2,1)}) %reduce-scatter.2.cloned.1.call-update) | async-done | bytes 1048592 | tf_op jit(solution)/shard_map/reduce_scatter | solution.py:153
  230.1 5.5 %all-to-all-start.1 = ((bf16[8,128,512]{2,1,0:T(8,128)(2,1)}), bf16[8,128,512]{2,1,0:T(8,128)(2,1)}, u32[]{:S(2)}, u32[]{:S(2)}) async-start(bf16[8,128,512]{2,1,0:T(8,128)(2,1)} %bitcast.65), calls=%async_computation.2 | async-start | bytes 2097152 | tf_op jit(solution)/shard_map/all_to_all | solution.py:156
  235.8 25.6 %all-to-all-done.1 = bf16[8,128,512]{2,1,0:T(8,128)(2,1)} async-done(((bf16[8,128,512]{2,1,0:T(8,128)(2,1)}), bf16[8,128,512]{2,1,0:T(8,128)(2,1)}, u32[]{:S(2)}, u32[]{:S(2)}) %all-to-all-start.1) | async-done | bytes 1048608 | tf_op jit(solution)/shard_map/all_to_all | solution.py:156
  261.4 3.3 %gather_fusion = bf16[512,512]{1,0:T(8,128)(2,1)S(1)} fusion(bf16[1024,512]{1,0:T(8,128)(2,1)} %bitcast.25, s32[1024]{0:T(1024)S(1)} %pad_clamp_fusion), kind=kCustom, calls=%fused_computation | custom fusion | bytes 1050624 | tf_op jit(solution)/shard_map/gather | solution.py:164
  264.7 1.6 reshape.465
  266.3 2.6 multiply_reduce_fusion
  268.9 1.7 add_convert_fusion.1
  (60 shorter events, 13.4 us)
Async XLA Ops:
  6.5 166.9 %copy-start = (bf16[1,640,2048]{2,1,0:T(8,128)(2,1)S(1)}, bf16[1,640,2048]{2,1,0:T(8,128)(2,1)}, u32[]{:S(2)}) copy-start(bf16[1,640,2048]{2,1,0:T(8,128)(2,1)} %param.23) | copy-start | bytes 7864324
  6.5 76.1 %all-reduce.2.cloned.1.call-start = ((), (), s32[]{:S(2)}) async-start(), calls=%async_computation.3 | async-start | bytes 2097152 | tf_op jit(solution)/shard_map/psum | solution.py:119
  9.1 22.7 %collective-permute-start = (bf16[128,256]{1,0:T(8,128)(2,1)}, bf16[128,256]{1,0:T(8,128)(2,1)}, u32[]{:S(2)}, u32[]{:S(2)}) collective-permute-start(bf16[128,256]{1,0:T(8,128)(2,1)} %get-tuple-element.21), channel_id=1, source_target_pairs={{0,4},{4,8},{8,12},{12,16},{16,20},{20,24},{24,28},{1,5},{5,9},{9,... | collective-permute-start | bytes 196616 | tf_op jit(solution)/shard_map/ppermute | solution.py:23
  14.6 17.2 %collective-permute-start.1 = (bf16[128,256]{1,0:T(8,128)(2,1)}, bf16[128,256]{1,0:T(8,128)(2,1)}, u32[]{:S(2)}, u32[]{:S(2)}) collective-permute-start(bf16[128,256]{1,0:T(8,128)(2,1)} %get-tuple-element.22), channel_id=1, source_target_pairs={{4,0},{8,4},{12,8},{16,12},{20,16},{24,20},{28,24},{5,1},{9,5},{13... | collective-permute-start | bytes 196616 | tf_op jit(solution)/shard_map/ppermute | solution.py:25
  33.6 1.8 copy-start.8
  35.4 1.9 copy-start.2
  38.4 3.6 %copy-start.3 = (bf16[512,2048]{1,0:T(8,128)(2,1)S(1)}, bf16[512,2048]{1,0:T(8,128)(2,1)}, u32[]{:S(2)}) copy-start(bf16[512,2048]{1,0:T(8,128)(2,1)} %param.17) | copy-start | bytes 6291460
  42.0 2.0 copy-start.6
  42.0 2.1 copy-start.7
  42.0 2.1 copy-start.5
  43.8 41.9 %copy-start.4 = (f32[2048]{0:T(1024)S(1)}, f32[2048]{0:T(1024)}, u32[]{:S(2)}) copy-start(f32[2048]{0:T(1024)} %param.18) | copy-start | bytes 24580
  43.8 121.6 %all-gather.2.cloned.1.call-start = ((), (), s32[]{:S(2)}) async-start(), calls=%async_computation.4 | async-start | bytes 5242880 | tf_op jit(solution)/shard_map/all_gather | solution.py:146
  84.7 1.0 copy-start.1
  131.9 98.2 %reduce-scatter.2.cloned.1.call-start = ((), (), s32[]{:S(2)}) async-start(), calls=%async_computation.5 | async-start | bytes 5242880 | tf_op jit(solution)/shard_map/reduce_scatter | solution.py:153
  185.5 50.1 %copy-start.9 = (f32[256,2]{0,1:T(2,128)S(1)}, f32[256,2]{0,1:T(2,128)}, u32[]{:S(2)}) copy-start(f32[256,2]{0,1:T(2,128)} %param.20) | copy-start | bytes 6148
  230.1 31.3 %all-to-all-start.1 = ((bf16[8,128,512]{2,1,0:T(8,128)(2,1)}), bf16[8,128,512]{2,1,0:T(8,128)(2,1)}, u32[]{:S(2)}, u32[]{:S(2)}) async-start(bf16[8,128,512]{2,1,0:T(8,128)(2,1)} %bitcast.65), calls=%async_computation.2 | async-start | bytes 2097152 | tf_op jit(solution)/shard_map/all_to_all | solution.py:156
Sparse Core Ops, SparseCore 0:
  43.9 38.7 all-reduce.1
  132.0 33.3 all-gather.1
  185.6 44.4 reduce-scatter.1
where the time goes:
time: 278 us; the launch traced here: 277 us
  waiting for transfers between devices  142 us (51%)
  local copies, waits for them, and re-layouts  32.3 us (12%)
  blocking collectives  30.7 us (11%)
  matrix products  27.1 us (10%)
  other arithmetic  19 us (7%)
  between operations  13.4 us (5%)
  starting transfers between devices  12.8 us (5%)
    reduce_scatter x1, waiting for transfers between devices, local(): lax.psum_scatter(partial_rows.astype(jnp.bfloat16), 'tp', scatter_dimensi...  44.6 us
    psum x1, waiting for transfers between devices, local(): lax.psum(partial_value.astype(jnp.bfloat16), 'tp').astype(jnp.float32)  38.5 us
    all_gather x1, waiting for transfers between devices, local(): joined_slots = lax.all_gather(arrived, 'tp', axis=1, tiled=True)  33.2 us
    all_to_all x1, blocking collectives, local(): lax.all_to_all(own_slots, 'sp', split_axis=0, concat_axis=0, tiled=True)  30.7 us
    all_to_all x1, waiting for transfers between devices, local(): lax.all_to_all(col_sums.reshape(sources, slot_count, col_width), 'sp', sp...  25.6 us
    dot_general x1, matrix products, local(): jnp.dot(hidden, w_down[0], preferred_element_type=jnp.float32)  12.1 us
    dot_general x1, matrix products, local(): up_part = jnp.dot(expert_rows, w_up[0], preferred_element_type=jnp.float32)  8 us
    scatter x1, local copies, waits for them, and re-layouts, local(): buffer = jnp.zeros((experts * capacity, width), jnp.bfloat16).at[destinat...  7.21 us
  transfers between devices with their start and end apart: 6, of which 4 were waited for; matrix products, arithmetic and copies ran while one was open for 6% of the time, Pallas kernels for 0%

commit v1 on v0

--- a/solution.py
+++ b/solution.py
@@ -1,6 +1,8 @@
 import jax
 import jax.numpy as jnp
 from jax import lax
+from jax.experimental import pallas as pl
+from jax.experimental.pallas import tpu as pltpu
 from jax.sharding import PartitionSpec as P
 
 HEAD_SIZE = 64
@@ -76,6 +78,400 @@
         "kgqj,jkd->qkgd", weights_bf, value_rows, preferred_element_type=jnp.float32
     )
     return mixed_heads.astype(jnp.bfloat16).reshape(query_rows.shape[0], -1)
+
+
+MESH = pl.DeviceIdType.MESH
+VMEM = pl.BlockSpec(memory_space=pltpu.VMEM)
+VMEM_LIMIT = 56 * 1024 * 1024
+
+
+def tp_places():
+    here = lax.axis_index("tp")
+    mate = here + 1 - 2 * lax.rem(here, 2)
+    across = lax.rem(here + 2, 4)
+    return here, mate, across
+
+
+def send(src, dst, send_sem, recv_sem, sp, tp):
+    return pltpu.make_async_remote_copy(
+        src_ref=src,
+        dst_ref=dst,
+        send_sem=send_sem,
+        recv_sem=recv_sem,
+        device_id=(sp, tp),
+        device_id_type=MESH,
+    )
+
+
+def shift_at(step, count):
+    return 1 + lax.rem(count // 2 - 1 + step, count - 1)
+
+
+def greet(count, me, here, mate, across):
+    barrier = pltpu.get_barrier_semaphore()
+
+    def signal(shift, carry):
+        pl.semaphore_signal(
+            barrier, inc=1, device_id=(lax.rem(me + shift, count), here), device_id_type=MESH
+        )
+        return carry
+
+    lax.fori_loop(1, count, signal, 0)
+    for other in (mate, across):
+        pl.semaphore_signal(barrier, inc=1, device_id=(me, other), device_id_type=MESH)
+    pl.semaphore_wait(barrier, count + 1)
+
+
+def project_dispatch_kernel(
+    count,
+    pieces,
+    partial,
+    residual,
+    gain,
+    places,
+    gathered,
+    stream_cols,
+    from_mate,
+    pair,
+    from_across,
+    stream,
+    normed,
+    own,
+    mate_sems,
+    across_sems,
+    back_sems,
+    slot_sems,
+    near_sems,
+    side_sems,
+    relay_sems,
+    local_sem,
+):
+    me = lax.axis_index("sp")
+    here, mate, across = tp_places()
+    half = partial.shape[0] // 2
+    rows = half // pieces
+    mine = pl.multiple_of(lax.rem(here, 2) * half, rows)
+    theirs = pl.multiple_of(half - mine, rows)
+    greet(count, me, here, mate, across)
+
+    def to_mate(i):
+        return send(
+            partial.at[pl.ds(theirs + i * rows, rows)], from_mate.at[pl.ds(i * rows, rows)],
+            mate_sems.at[0, i], mate_sems.at[1, i], me, mate,
+        )
+
+    def to_across(i):
+        return send(
+            pair.at[pl.ds(i * rows, rows)], from_across.at[pl.ds(i * rows, rows)],
+            across_sems.at[0, i], across_sems.at[1, i], me, across,
+        )
+
+    def to_back(i, start):
+        part = stream.at[pl.ds(start + i * rows, rows)]
+        return send(part, part, back_sems.at[0, i], back_sems.at[1, i], me, mate)
+
+    def normalise(at):
+        x = stream[at, :].astype(jnp.float32)
+        scale = lax.rsqrt(jnp.mean(x * x, axis=-1, keepdims=True) + NORM_EPS)
+        normed[at, :] = (x * scale * gain[...]).astype(jnp.bfloat16)
+
+    for i in range(pieces):
+        to_mate(i).start()
+    for i in range(pieces):
+        to_mate(i).wait_recv()
+        at = pl.ds(i * rows, rows)
+        pair[at, :] = (
+            partial[pl.ds(mine + i * rows, rows), :].astype(jnp.float32)
+            + from_mate[at, :].astype(jnp.float32)
+        ).astype(jnp.bfloat16)
+        to_across(i).start()
+    for i in range(pieces):
+        to_across(i).wait_recv()
+        at = pl.ds(i * rows, rows)
+        full = pl.ds(mine + i * rows, rows)
+        stream[full, :] = (
+            residual[full, :].astype(jnp.float32)
+            + (pair[at, :].astype(jnp.float32) + from_across[at, :].astype(jnp.float32))
+        ).astype(jnp.bfloat16)
+        to_back(i, mine).start()
+        normalise(full)
+    for i in range(pieces):
+        to_back(i, theirs).wait_recv()
+        normalise(pl.ds(theirs + i * rows, rows))
+    width = stream_cols.shape[1]
+    stream_cols[...] = stream[:, pl.ds(pl.multiple_of(here * width, 128), width)]
+    quarter = own.shape[1]
+    rowid = lax.broadcasted_iota(jnp.int32, (count * quarter, places.shape[1]), 0)
+    chosen = (rowid == places[0:1, :]) | (rowid == places[1:2, :])
+    chosen = jnp.where(chosen, 1.0, 0.0).astype(jnp.bfloat16)
+    picked = jnp.dot(chosen, normed[...], preferred_element_type=jnp.float32).astype(jnp.bfloat16)
+    for e in range(count):
+        own[e] = picked[e * quarter : (e + 1) * quarter, :]
+
+    def to_expert(k):
+        return send(
+            own.at[lax.rem(me + k, count)], gathered.at[me, here],
+            slot_sems.at[0, k], slot_sems.at[1, k], lax.rem(me + k, count), here,
+        )
+
+    def source(k):
+        return lax.rem(me - k + count, count)
+
+    def to_near(k, src):
+        return send(
+            src, gathered.at[source(k), here],
+            near_sems.at[0, k], near_sems.at[1, k], me, mate,
+        )
+
+    def to_side(k, src):
+        return send(
+            src, gathered.at[source(k), here],
+            side_sems.at[0, k], side_sems.at[1, k], me, across,
+        )
+
+    def to_relay(k):
+        part = gathered.at[source(k), across]
+        return send(part, part, relay_sems.at[0, k], relay_sems.at[1, k], me, mate)
+
+    kept = pltpu.make_async_copy(own.at[me], gathered.at[me, here], local_sem)
+    kept.start()
+
+    def start_slot(j, carry):
+        to_expert(shift_at(j, count)).start()
+        return carry
+
+    to_side(0, own.at[me]).start()
+    lax.fori_loop(0, count - 1, start_slot, 0)
+    to_near(0, own.at[me]).start()
+
+    def landed(k):
+        return gathered.at[source(k), here]
+
+    def pass_on(j, last):
+        k = shift_at(j, count)
+        to_expert(k).wait_recv()
+        to_side(k, landed(k)).start()
+        to_near(k, landed(k)).start()
+        to_side(last, landed(last)).wait_recv()
+        to_relay(last).start()
+        return k
+
+    last = lax.fori_loop(0, count - 1, pass_on, 0)
+    to_side(last, landed(last)).wait_recv()
+    to_relay(last).start()
+
+    def finish(k, carry):
+        to_near(k, landed(k)).wait()
+        to_relay(k).wait()
+        to_side(k, landed(k)).wait_send()
+        return carry
+
+    lax.fori_loop(0, count, finish, 0)
+
+    def finish_slot(k, carry):
+        to_expert(k).wait_send()
+        return carry
+
+    lax.fori_loop(1, count, finish_slot, 0)
+    kept.wait()
+    for i in range(pieces):
+        to_mate(i).wait_send()
+        to_across(i).wait_send()
+        to_back(i, mine).wait_send()
+
+
+def project_dispatch(partial, residual, gain, places, count, quarter, cols, pieces):
+    rows, width = partial.shape
+    half = rows // 2
+    dma = pltpu.SemaphoreType.DMA
+    bf = jnp.bfloat16
+    return pl.pallas_call(
+        lambda *refs: project_dispatch_kernel(count, pieces, *refs),
+        out_shape=(
+            jax.ShapeDtypeStruct((count, 4, quarter, width), bf),
+            jax.ShapeDtypeStruct((rows, cols), bf),
+        ),
+        in_specs=[VMEM] * 4,
+        out_specs=(VMEM, VMEM),
+        scratch_shapes=[
+            pltpu.VMEM((half, width), bf),
+            pltpu.VMEM((half, width), bf),
+            pltpu.VMEM((half, width), bf),
+            pltpu.VMEM((rows, width), bf),
+            pltpu.VMEM((rows, width), bf),
+            pltpu.VMEM((count, quarter, width), bf),
+            dma((2, pieces)),
+            dma((2, pieces)),
+            dma((2, pieces)),
+            dma((2, count)),
+            dma((2, count)),
+            dma((2, count)),
+            dma((2, count)),
+            dma,
+        ],
+        compiler_params=pltpu.CompilerParams(
+            collective_id=0, has_side_effects=True, vmem_limit_bytes=VMEM_LIMIT
+        ),
+    )(partial, residual, gain, places)
+
+
+def combine_kernel(
+    count,
+    partial,
+    stream_cols,
+    target,
+    weight,
+    out,
+    from_mate,
+    pair,
+    from_across,
+    total,
+    back,
+    mix,
+    mate_sems,
+    across_sems,
+    back_sems,
+    local_sem,
+):
+    me = lax.axis_index("sp")
+    here, mate, across = tp_places()
+    cols = out.shape[1]
+    slots = partial.shape[1]
+    greet(count, me, here, mate, across)
+
+    def block(which):
+        return pl.ds(pl.multiple_of(which * cols, 128), cols)
+
+    def dest(k):
+        return lax.rem(me + k, count)
+
+    def order(j):
+        return lax.rem(count // 2 + j, count)
+
+    def to_mate(k, part):
+        cb = mate if part == 0 else lax.rem(mate + 2, 4)
+        return send(
+            partial.at[dest(k), :, block(cb)], from_mate.at[dest(k), part],
+            mate_sems.at[0, part, k], mate_sems.at[1, part, k], me, mate,
+        )
+
+    def to_across(k):
+        return send(
+            pair.at[dest(k)], from_across.at[dest(k)],
+            across_sems.at[0, k], across_sems.at[1, k], me, across,
+        )
+
+    def to_back(k):
+        return send(
+            total.at[dest(k)], back.at[me], back_sems.at[0, k], back_sems.at[1, k], dest(k), here
+        )
+
+    def start_mate(j, carry):
+        to_mate(order(j), 1).start()
+        to_mate(order(j), 0).start()
+        return carry
+
+    lax.fori_loop(0, count, start_mate, 0)
+
+    def start_across(j, carry):
+        k = order(j)
+        to_mate(k, 1).wait_recv()
+        pair[dest(k)] = (
+            partial[dest(k), :, block(across)].astype(jnp.float32)
+            + from_mate[dest(k), 1].astype(jnp.float32)
+        ).astype(jnp.bfloat16)
+        to_across(k).start()
+        return carry
+
+    lax.fori_loop(0, count, start_across, 0)
+
+    def start_back(j, carry):
+        k = order(j)
+        to_mate(k, 0).wait_recv()
+        to_across(k).wait_recv()
+        total[dest(k)] = (
+            partial[dest(k), :, block(here)].astype(jnp.float32)
+            + from_mate[dest(k), 0].astype(jnp.float32)
+            + from_across[dest(k)].astype(jnp.float32)
+        ).astype(jnp.bfloat16)
+
+        @pl.when(k != 0)
+        def _():
+            to_back(k).start()
+
+        return carry
+
+    lax.fori_loop(0, count, start_back, 0)
+    kept = pltpu.make_async_copy(total.at[me], back.at[me], local_sem)
+    kept.start()
+    mix[...] = jnp.zeros_like(mix)
+    slot_ids = lax.broadcasted_iota(jnp.int32, (out.shape[0], slots), 1)
+
+    def add(expert):
+        ids = slot_ids + expert * slots
+        table = jnp.where(ids == target[:, 0:1], weight[:, 0:1], 0.0) + jnp.where(
+            ids == target[:, 1:2], weight[:, 1:2], 0.0
+        )
+        high = table.astype(jnp.bfloat16)
+        low = (table - high.astype(jnp.float32)).astype(jnp.bfloat16)
+        rows = back[expert]
+        mix[...] += jnp.dot(high, rows, preferred_element_type=jnp.float32) + jnp.dot(
+            low, rows, preferred_element_type=jnp.float32
+        )
+
+    kept.wait()
+    add(me)
+
+    def receive(j, carry):
+        k = shift_at(j, count)
+        to_back(k).wait_recv()
+        add(lax.rem(me - k + count, count))
+        return carry
+
+    lax.fori_loop(0, count - 1, receive, 0)
+    out[...] = (stream_cols[...].astype(jnp.float32) + mix[...]).astype(jnp.bfloat16)
+
+    def finish(k, carry):
+        to_mate(k, 0).wait_send()
+        to_mate(k, 1).wait_send()
+        to_across(k).wait_send()
+        return carry
+
+    lax.fori_loop(0, count, finish, 0)
+
+    def finish_back(k, carry):
+        to_back(k).wait_send()
+        return carry
+
+    lax.fori_loop(1, count, finish_back, 0)
+
+
+def combine(partial, stream_cols, target, weight):
+    count, slots, _ = partial.shape
+    cols = stream_cols.shape[1]
+    dma = pltpu.SemaphoreType.DMA
+    bf = jnp.bfloat16
+    return pl.pallas_call(
+        lambda *refs: combine_kernel(count, *refs),
+        out_shape=jax.ShapeDtypeStruct(stream_cols.shape, bf),
+        in_specs=[VMEM] * 4,
+        out_specs=VMEM,
+        scratch_shapes=[
+            pltpu.VMEM((count, 2, slots, cols), bf),
+            pltpu.VMEM((count, slots, cols), bf),
+            pltpu.VMEM((count, slots, cols), bf),
+            pltpu.VMEM((count, slots, cols), bf),
+            pltpu.VMEM((count, slots, cols), bf),
+            pltpu.VMEM(stream_cols.shape, jnp.float32),
+            dma((2, 2, count)),
+            dma((2, count)),
+            dma((2, count)),
+            dma,
+        ],
+        compiler_params=pltpu.CompilerParams(
+            collective_id=1, has_side_effects=True, vmem_limit_bytes=VMEM_LIMIT
+        ),
+    )(partial, stream_cols, target, weight)
 
 
 def local(
@@ -115,58 +511,32 @@
     width = partial_value.shape[1]
     col_blocks = lax.axis_size("tp")
     col_width = width // col_blocks
-    col_start = lax.axis_index("tp") * col_width
-    summed = lax.psum(partial_value.astype(jnp.bfloat16), "tp").astype(jnp.float32)
-    stream = (residual.astype(jnp.float32) + summed).astype(jnp.bfloat16)
-    as_float = stream.astype(jnp.float32)
-    normed = (
-        as_float
-        * lax.rsqrt(jnp.mean(as_float * as_float, axis=-1, keepdims=True) + NORM_EPS)
-        * norm_gain
-    ).astype(jnp.bfloat16)
-    stream_cols = lax.dynamic_slice_in_dim(stream, col_start, col_width, 1)
     top_count = routes.shape[1]
     experts = w_gate.shape[0] * seq_devices
     capacity = 2 * top_count * tok_rows // experts
-    flat_routes = routes.reshape(-1)
-    onehot = (flat_routes[:, None] == jnp.arange(experts, dtype=jnp.int32)[None, :]).astype(
-        jnp.int32
-    )
-    slot_number = jnp.sum(jnp.cumsum(onehot, axis=0) * onehot, axis=1) - 1
-    destination = flat_routes * capacity + slot_number
-    buffer = (
-        jnp.zeros((experts * capacity, width), jnp.bfloat16)
-        .at[destination]
-        .set(jnp.repeat(normed, top_count, axis=0))
-        .reshape(experts, capacity, width)
-    )
     quarter = capacity // col_blocks
-    own_slots = lax.dynamic_slice_in_dim(buffer, lax.axis_index("tp") * quarter, quarter, 1)
-    arrived = lax.all_to_all(own_slots, "sp", split_axis=0, concat_axis=0, tiled=True)
-    joined_slots = lax.all_gather(arrived, "tp", axis=1, tiled=True)
-    sources, slot_count, _ = joined_slots.shape
-    expert_rows = joined_slots.reshape(-1, width)
+    expert_ids = jnp.arange(experts, dtype=jnp.int32)
+    named = routes[:, :, None] == expert_ids
+    counted = jnp.any(named, axis=1).astype(jnp.bfloat16)
+    earlier = jnp.tri(tok_rows, k=-1, dtype=jnp.bfloat16)
+    before = jnp.dot(earlier, counted, preferred_element_type=jnp.float32)
+    slot_number = jnp.sum(jnp.where(named, before[:, None, :], 0.0), axis=2).astype(jnp.int32)
+    destination = routes * capacity + slot_number
+    inside = slot_number - lax.axis_index("tp") * quarter
+    places = jnp.where((inside >= 0) & (inside < quarter), routes * quarter + inside, -1).T
+    gathered, stream_cols = project_dispatch(
+        partial_value.astype(jnp.bfloat16), residual, norm_gain[None, :], places,
+        seq_devices, quarter, col_width, 4,
+    )
+    expert_rows = gathered.reshape(-1, width)
     gate_part = jnp.dot(expert_rows, w_gate[0], preferred_element_type=jnp.float32)
     up_part = jnp.dot(expert_rows, w_up[0], preferred_element_type=jnp.float32)
     hidden = (jax.nn.silu(gate_part) * up_part).astype(jnp.bfloat16)
     partial_rows = jnp.dot(hidden, w_down[0], preferred_element_type=jnp.float32)
-    col_sums = lax.psum_scatter(
-        partial_rows.astype(jnp.bfloat16), "tp", scatter_dimension=1, tiled=True
-    )
-    returned = lax.all_to_all(
-        col_sums.reshape(sources, slot_count, col_width),
-        "sp",
-        split_axis=0,
-        concat_axis=0,
-        tiled=True,
-    )
-    picked = (
-        returned.reshape(-1, col_width)[destination]
-        .astype(jnp.float32)
-        .reshape(tok_rows, top_count, col_width)
-    )
-    mixture = jnp.sum(picked * route_weights[:, :, None], axis=1)
-    return (stream_cols.astype(jnp.float32) + mixture).astype(jnp.bfloat16)
+    return combine(
+        partial_rows.astype(jnp.bfloat16).reshape(seq_devices, capacity, width),
+        stream_cols, destination, route_weights,
+    )
 
 
 def solution(mesh):

time: 278 us -> 162 us (0.58)
  waiting for transfers between devices: 142 us -> 0.01 us
  Pallas kernels: 0 us -> 104 us
  blocking collectives: 30.7 us -> 0 us
  local copies, waits for them, and re-layouts: 32.3 us -> 10.4 us
  between operations: 13.4 us -> 0.16 us
  other arithmetic: 19 us -> 12.5 us
  starting transfers between devices: 12.8 us -> 6.8 us
    pallas_call x0 -> x2, Pallas kernels: none -> 104 us  [the longest x1 57.7 us: project_dispatch(): pl.pallas_call(lambda *refs: project_dispatch_kernel(count, pieces, *refs...]
    reduce_scatter x1 -> x0, waiting for transfers between devices: 44.6 us -> none  [local(): lax.psum_scatter(partial_rows.astype(jnp.bfloat16), 'tp', scatter_dimensi...]
    psum x1 -> x0, waiting for transfers between devices: 38.5 us -> none  [local(): lax.psum(partial_value.astype(jnp.bfloat16), 'tp').astype(jnp.float32)]
    all_gather x1 -> x0, waiting for transfers between devices: 33.2 us -> none  [local(): joined_slots = lax.all_gather(arrived, 'tp', axis=1, tiled=True)]
    all_to_all x1 -> x0, blocking collectives: 30.7 us -> none  [local(): lax.all_to_all(own_slots, 'sp', split_axis=0, concat_axis=0, tiled=True)]
    all_to_all x1 -> x0, waiting for transfers between devices: 25.6 us -> none  [local(): lax.all_to_all(col_sums.reshape(sources, slot_count, col_width), 'sp', sp...]
    scatter x1 -> x0, local copies, waits for them, and re-layouts: 7.21 us -> none  [local(): buffer = jnp.zeros((experts * capacity, width), jnp.bfloat16).at[destinat...]
    all_to_all x1 -> x0, starting transfers between devices: 5.52 us -> none  [local(): lax.all_to_all(col_sums.reshape(sources, slot_count, col_width), 'sp', sp...]
  transfers between devices with their start and end apart: 6 -> 2, of which waited for: 4 -> 0; matrix products, arithmetic and copies ran while one was open for 6% -> 9% of each run, Pallas kernels for 0% -> 0%
where the time goes in v1:
time: 162 us; the launch traced here: 161 us
  Pallas kernels  104 us (64%)
  matrix products  27.1 us (17%)
  other arithmetic  12.5 us (8%)
  local copies, waits for them, and re-layouts  10.4 us (6%)
  starting transfers between devices  6.8 us (4%)
    pallas_call x1, Pallas kernels, project_dispatch(): pl.pallas_call(lambda *refs: project_dispatch_kernel(count, pieces, *refs...  57.7 us
    pallas_call x1, Pallas kernels, combine(): pl.pallas_call(lambda *refs: combine_kernel(count, *refs), out_shape=jax....  46.5 us
    dot_general x1, matrix products, local(): jnp.dot(hidden, w_down[0], preferred_element_type=jnp.float32)  12.1 us
    dot_general x1, matrix products, local(): up_part = jnp.dot(expert_rows, w_up[0], preferred_element_type=jnp.float32)  7.17 us
    unnamed x12, local copies, waits for them, and re-layouts  7.1 us
    ppermute x1, starting transfers between devices, padded(): lax.ppermute(tail, axis, [(i, (i + 1) % count) for i in range(ends)])  5.52 us
    dot_general x1, matrix products, attend_block(): jnp.einsum('kgqj,jkd->qkgd', weights_bf, value_rows, preferred_element_ty...  3.54 us
  transfers between devices with their start and end apart: 2, of which 0 were waited for; matrix products, arithmetic and copies ran while one was open for 9% of the time, Pallas kernels for 0%

profile of v1, /device:TPU:0, one launch (start us, length us, event | category | flops | bytes accessed | tf_op | source)
XLA Modules:
  0.0 161.3 jit_solution(531883781072112861)
XLA Ops:
  0.0 1.0 constant_dynamic-update-slice_fusion.1
  1.0 0.9 constant_dynamic-update-slice_fusion
  1.9 0.7 fusion.47
  2.5 5.5 %collective-permute-start = (bf16[128,256]{1,0:T(8,128)(2,1)}, bf16[128,256]{1,0:T(8,128)(2,1)}, u32[]{:S(2)}, u32[]{:S(2)}) collective-permute-start(bf16[128,256]{1,0:T(8,128)(2,1)} %get-tuple-element.23), channel_id=1, source_target_pairs={{0,4},{4,8},{8,12},{12,16},{16,20},{20,24},{24,28},{1,5},{5,9},{9,... | collective-permute-start | bytes 196616 | tf_op jit(solution)/shard_map/ppermute | solution.py:25
  8.1 1.3 collective-permute-start.1
  9.9 0.6 fusion.40
  11.0 0.6 fusion.36
  11.6 0.6 iota_add_fusion.1
  12.2 1.1 copy.54
  13.3 0.7 fusion.31
  14.0 0.9 fusion.23
  14.9 0.7 select_reduce_fusion
  15.6 1.5 multiply_cosine_fusion.1
  17.2 0.9 multiply_cosine_fusion.3
  18.1 1.0 fusion.14
  19.0 0.8 subtract_convert_fusion.1
  19.8 1.3 multiply_add_fusion
  21.1 0.7 max.18
  21.8 0.8 copy.56.refs_2_
  22.6 1.5 copy.57.refs_3_
  24.1 0.9 pad_maximum_fusion
  25.2 0.8 subtract_convert_fusion.3
  26.0 1.7 %fusion.1 = (f32[2,4,256]{2,1,0:T(4,128)S(1)}, f32[2,512,256,4]{2,1,3,0:T(8,128)S(1)}) fusion(pred[256,512]{0,1:T(8,128)(4,1)S(1)} %fusion.14, bf16[256,2,4,16]{0,3,2,1:T(8,128)(2,1)} %bitcast.64, bf16[256,2,4,16]{0,3,2,1:T(8,128)(2,1)} %bitcast.65, bf16[256,2,4,16]{0,3,2,1:T(8,128)(2,1)} %bitcast.63, bf16[256,2,4,16]{0,3,2,1:T(8,128)(2,1)} %bitcast.62, ...), kind=kOutput, calls=%fused_computation.5 | convolution fusion | flops 138934272 | bytes 4726784 | tf_op jit(solution)/shard_map/qkgd,jkd->kgqj/dot_general | solution.py:63
  27.9 1.9 %copy-done.1 = f32[2,512,256,4]{2,1,3,0:T(8,128)} copy-done((f32[2,512,256,4]{2,1,3,0:T(8,128)}, f32[2,512,256,4]{2,1,3,0:T(8,128)S(1)}, u32[]{:S(2)}) %copy-start.1) | copy-done | bytes 4194328
  29.7 0.9 fusion
  30.8 3.5 %fusion.10 = bf16[2,64,4,256]{3,1,2,0:T(8,128)(2,1)S(1)} fusion(bf16[512,2,64,1]{0,2,3,1:T(8,128)(2,1)S(1)} %bitcast.61, f32[2,512,256,4]{2,1,3,0:T(8,128)} %copy-done.1, f32[2,4,256]{2,1,0:T(4,128)S(1)} %exponential_add_fusion, f32[2,4,256]{2,1,0:T(4,128)S(1)} %broadcast_maximum_fusion, pred[256,512]{0,1:T(8,128)(4,1)S(1)} %fusion.14), kind=kOutput, calls=%fused_computation.14 | convolution fusion | flops 139591680 | bytes 4734976 | tf_op jit(solution)/shard_map/kgqj,jkd->qkgd/dot_general | solution.py:77
  34.4 1.7 %convolution_convert_fusion.1.refs_0_ = bf16[256,2048]{1,0:T(8,128)(2,1)} fusion(bf16[256,512]{0,1:T(8,128)(2,1)S(1)} %bitcast.60, bf16[512,2048]{1,0:T(8,128)(2,1)S(1)} %copy-done.2), kind=kOutput, calls=%fused_computation.12 | convolution fusion | flops 537395200 | bytes 3407872 | tf_op jit(solution)/shard_map/dot_general | solution.py:510
  36.1 57.7 %shard_map.118 = (bf16[8,4,32,2048]{3,2,1,0:T(8,128)(2,1)}, bf16[256,512]{1,0:T(8,128)(2,1)}) custom-call(bf16[256,2048]{1,0:T(8,128)(2,1)} %convolution_convert_fusion.1.refs_0_, bf16[256,2048]{1,0:T(8,128)(2,1)} %refs_1_.1, f32[1,2048]{1,0:T(1,128)} %bitcast.66, s32[2,256]{1,0:T(2,128)} %get-tuple-element.26.refs_3_), custom_call_target="tpu_custom_call" | custom-call | tf_op jit(solution)/shard_map/pallas_call | solution.py:288
  93.8 7.2 %fusion.3 = f32[1024,640]{1,0:T(8,128)} fusion(bf16[1024,2048]{1,0:T(8,128)(2,1)} %bitcast.67, bf16[1,2048,640]{2,1,0:T(8,128)(2,1)S(1)} %copy-done.3), kind=kOutput, calls=%fused_computation.7 | convolution fusion | flops 2684354560 | bytes 9437184 | tf_op jit(solution)/shard_map/dot_general | solution.py:533
  101.0 12.1 %convolution_convert_fusion = bf16[1024,2048]{1,0:T(8,128)(2,1)} fusion(bf16[1,640,2048]{2,1,0:T(8,128)(2,1)S(1)} %copy-done, f32[1024,640]{1,0:T(8,128)} %fusion.3, bf16[1024,2048]{1,0:T(8,128)(2,1)} %bitcast.68, bf16[1,2048,640]{2,1,0:T(8,128)(2,1)} %param.21), kind=kOutput, calls=%fused_computation.3 | convolution fusion | flops 5374738432 | bytes 16252928 | tf_op jit(solution)/shard_map/dot_general | solution.py:535
  113.1 46.5 %shard_map.119 = bf16[256,512]{1,0:T(8,128)(2,1)} custom-call(bf16[8,128,2048]{2,1,0:T(8,128)(2,1)} %bitcast.57, bf16[256,512]{1,0:T(8,128)(2,1)} %get-tuple-element.8.refs_1_, s32[256,2]{1,0:T(8,128)} %copy.56.refs_2_, f32[256,2]{1,0:T(8,128)} %copy.57.refs_3_), custom_call_target="tpu_custom_call" | custom-call | tf_op jit(solution)/shard_map/pallas_call | solution.py:454
  159.6 1.7 %copy.63 = bf16[256,512]{1,0:T(8,128)(2,1)} copy(bf16[256,512]{1,0:T(8,128)(2,1)} %shard_map.119) | data formatting | bytes 524288
  (19 shorter events, 1.6 us)
Async XLA Ops:
  0.0 101.0 %copy-start = (bf16[1,640,2048]{2,1,0:T(8,128)(2,1)S(1)}, bf16[1,640,2048]{2,1,0:T(8,128)(2,1)}, u32[]{:S(2)}) copy-start(bf16[1,640,2048]{2,1,0:T(8,128)(2,1)} %param.23) | copy-start | bytes 7864324
  2.5 21.6 %collective-permute-start = (bf16[128,256]{1,0:T(8,128)(2,1)}, bf16[128,256]{1,0:T(8,128)(2,1)}, u32[]{:S(2)}, u32[]{:S(2)}) collective-permute-start(bf16[128,256]{1,0:T(8,128)(2,1)} %get-tuple-element.23), channel_id=1, source_target_pairs={{0,4},{4,8},{8,12},{12,16},{16,20},{20,24},{24,28},{1,5},{5,9},{9,... | collective-permute-start | bytes 196616 | tf_op jit(solution)/shard_map/ppermute | solution.py:25
  8.1 16.0 %collective-permute-start.1 = (bf16[128,256]{1,0:T(8,128)(2,1)}, bf16[128,256]{1,0:T(8,128)(2,1)}, u32[]{:S(2)}, u32[]{:S(2)}) collective-permute-start(bf16[128,256]{1,0:T(8,128)(2,1)} %get-tuple-element.24), channel_id=1, source_target_pairs={{4,0},{8,4},{12,8},{16,12},{20,16},{24,20},{28,24},{5,1},{9,5},{13... | collective-permute-start | bytes 196616 | tf_op jit(solution)/shard_map/ppermute | solution.py:27
  27.8 1.9 %copy-start.1 = (f32[2,512,256,4]{2,1,3,0:T(8,128)}, f32[2,512,256,4]{2,1,3,0:T(8,128)S(1)}, u32[]{:S(2)}) copy-start(f32[2,512,256,4]{2,1,3,0:T(8,128)S(1)} %get-tuple-element.40) | copy-start | bytes 12582916
  30.8 3.6 %copy-start.2 = (bf16[512,2048]{1,0:T(8,128)(2,1)S(1)}, bf16[512,2048]{1,0:T(8,128)(2,1)}, u32[]{:S(2)}) copy-start(bf16[512,2048]{1,0:T(8,128)(2,1)} %param.17) | copy-start | bytes 6291460
  34.4 59.4 %copy-start.3 = (bf16[1,2048,640]{2,1,0:T(8,128)(2,1)S(1)}, bf16[1,2048,640]{2,1,0:T(8,128)(2,1)}, u32[]{:S(2)}) copy-start(bf16[1,2048,640]{2,1,0:T(8,128)(2,1)} %param.22) | copy-start | bytes 7864324

commit v2 on v1

--- a/solution.py
+++ b/solution.py
@@ -12,72 +12,6 @@
 
 ROPE_BASE = 10000.0
 NORM_EPS = 1e-06
-
-
-def padded(cells, sides, width):
-    for axis, dim in sides:
-        count = lax.axis_size(axis)
-        ends = count - 1
-        head = lax.slice_in_dim(cells, 0, width, axis=dim)
-        tail = lax.slice_in_dim(cells, cells.shape[dim] - width, cells.shape[dim], axis=dim)
-        cells = jnp.concatenate(
-            [
-                lax.ppermute(tail, axis, [(i, (i + 1) % count) for i in range(ends)]),
-                cells,
-                lax.ppermute(head, axis, [((i + 1) % count, i) for i in range(ends)]),
-            ],
-            axis=dim,
-        )
-    return cells
-
-
-def rotate_pair(values_half, angles):
-    first_half, second = jnp.split(values_half, 2, axis=-1)
-    cosine = jnp.cos(angles)[:, None, :]
-    sine_part = jnp.sin(angles)[:, None, :]
-    return jnp.concatenate(
-        [first_half * cosine - second * sine_part, second * cosine + first_half * sine_part],
-        axis=-1,
-    )
-
-
-def axial_rotation(heads_in, token_positions):
-    half_dim = HEAD_SIZE // 2
-    inverse = ROPE_BASE ** (-jnp.arange(0, half_dim, 2, dtype=jnp.float32) / half_dim)
-    row_angles = (token_positions // GRID_W).astype(jnp.float32)[:, None] * inverse
-    col_angles = (token_positions % GRID_W).astype(jnp.float32)[:, None] * inverse
-    as_float = heads_in.astype(jnp.float32)
-    return jnp.concatenate(
-        [
-            rotate_pair(as_float[..., :half_dim], row_angles),
-            rotate_pair(as_float[..., half_dim:], col_angles),
-        ],
-        axis=-1,
-    )
-
-
-def attend_block(query_rows, key_rows, value_rows, sink_logit, query_pos, key_pos, total_rows):
-    kv_heads = key_rows.shape[1]
-    groups = query_rows.shape[1] // kv_heads
-    grouped = query_rows.reshape(query_rows.shape[0], kv_heads, groups, HEAD_SIZE)
-    scores = jnp.einsum(
-        "qkgd,jkd->kgqj", grouped, key_rows, preferred_element_type=jnp.float32
-    ) * HEAD_SIZE ** (-0.5)
-    in_window = (
-        (jnp.abs(key_pos[None, :] - query_pos[:, None]) <= WINDOW)
-        & (key_pos[None, :] >= 0)
-        & (key_pos[None, :] < total_rows)
-    )
-    scores = jnp.where(in_window[None, None], scores, -jnp.inf)
-    sink_col = sink_logit.reshape(kv_heads, groups, 1, 1)
-    largest = jnp.maximum(jnp.max(scores, axis=-1, keepdims=True), sink_col)
-    exp_scores = jnp.exp(scores - largest)
-    denominator = jnp.sum(exp_scores, axis=-1, keepdims=True) + jnp.exp(sink_col - largest)
-    weights_bf = (exp_scores / denominator).astype(jnp.bfloat16)
-    mixed_heads = jnp.einsum(
-        "kgqj,jkd->qkgd", weights_bf, value_rows, preferred_element_type=jnp.float32
-    )
-    return mixed_heads.astype(jnp.bfloat16).reshape(query_rows.shape[0], -1)
 
 
 MESH = pl.DeviceIdType.MESH
@@ -125,12 +59,34 @@
 def project_dispatch_kernel(
     count,
     pieces,
+    sinks,
+    query,
+    keys,
+    values,
+    row_turn,
+    col_turn,
+    swap,
+    gain,
+    routes,
+    w_out_hbm,
+    residual_hbm,
+    w_gate_hbm,
+    w_up_hbm,
+    hidden,
+    stream_cols,
+    target,
+    gathered,
+    w_gate,
+    w_up,
+    key_wide,
+    value_wide,
+    key_twice,
+    value_twice,
+    turned,
+    attended,
+    w_out,
+    residual,
     partial,
-    residual,
-    gain,
-    places,
-    gathered,
-    stream_cols,
     from_mate,
     pair,
     from_across,
@@ -145,6 +101,8 @@
     side_sems,
     relay_sems,
     local_sem,
+    halo_sems,
+    load_sems,
 ):
     me = lax.axis_index("sp")
     here, mate, across = tp_places()
@@ -152,7 +110,125 @@
     rows = half // pieces
     mine = pl.multiple_of(lax.rem(here, 2) * half, rows)
     theirs = pl.multiple_of(half - mine, rows)
+    loads = [
+        pltpu.make_async_copy(w_out_hbm, w_out, load_sems.at[0]),
+        pltpu.make_async_copy(residual_hbm, residual, load_sems.at[1]),
+        pltpu.make_async_copy(w_gate_hbm, w_gate, load_sems.at[2]),
+        pltpu.make_async_copy(w_up_hbm, w_up, load_sems.at[3]),
+    ]
+    for load in loads:
+        load.start()
     greet(count, me, here, mate, across)
+    tokens = query.shape[0]
+    up, down = me + 1, me - 1
+    low, high = pl.ds(0, WINDOW), pl.ds(tokens + WINDOW, WINDOW)
+    pairs = ((keys, key_wide), (values, value_wide))
+
+    def halo(which, upward):
+        raw, wide = pairs[which]
+        if upward:
+            src, dst, sp = raw.at[pl.ds(tokens - WINDOW, WINDOW)], wide.at[low], up
+        else:
+            src, dst, sp = raw.at[pl.ds(0, WINDOW)], wide.at[high], down
+        way = 1 if upward else 0
+        return send(src, dst, halo_sems.at[0, which, way], halo_sems.at[1, which, way], sp, here)
+
+    @pl.when(me < count - 1)
+    def _():
+        halo(0, True).start()
+        halo(1, True).start()
+
+    @pl.when(me > 0)
+    def _():
+        halo(0, False).start()
+        halo(1, False).start()
+
+    lane = lax.broadcasted_iota(jnp.int32, (1, 128), 1)
+    by_row = lax.rem(lane, HEAD_SIZE) < HEAD_SIZE // 2
+    left = lane < HEAD_SIZE
+    edge = WINDOW // GRID_W
+
+    def turn(x, grid_row):
+        cosine = jnp.where(by_row, row_turn[0, grid_row : grid_row + 1, :], col_turn[0])
+        sine = jnp.where(by_row, row_turn[1, grid_row : grid_row + 1, :], col_turn[1])
+        swapped = jnp.dot(x, swap[...], preferred_element_type=jnp.float32)
+        return (x.astype(jnp.float32) * cosine + swapped * sine).astype(jnp.bfloat16)
+
+    def twice(x, place, at):
+        other = pltpu.roll(x.astype(jnp.float32), HEAD_SIZE, 1).astype(jnp.bfloat16)
+        place[0, at, :] = jnp.where(left, x, other)
+        place[1, at, :] = jnp.where(left, other, x)
+
+    for r in range(tokens // GRID_W):
+        at = pl.ds(r * GRID_W, GRID_W)
+        for j in range(query.shape[1] // 128):
+            block = pl.ds(j * 128, 128)
+            turned[at, block] = turn(query[at, block], r + edge) * HEAD_SIZE**-0.5
+        wide_at = pl.ds(WINDOW + r * GRID_W, GRID_W)
+        twice(turn(keys[at, :], r + edge), key_twice, wide_at)
+        twice(values[at, :], value_twice, wide_at)
+
+    @pl.when(me > 0)
+    def _():
+        halo(0, True).wait_recv()
+        halo(1, True).wait_recv()
+
+    @pl.when(me == 0)
+    def _():
+        key_wide[low, :] = jnp.zeros((WINDOW, 128), jnp.bfloat16)
+        value_wide[low, :] = jnp.zeros((WINDOW, 128), jnp.bfloat16)
+
+    @pl.when(me < count - 1)
+    def _():
+        halo(0, False).wait_recv()
+        halo(1, False).wait_recv()
+
+    @pl.when(me == count - 1)
+    def _():
+        key_wide[high, :] = jnp.zeros((WINDOW, 128), jnp.bfloat16)
+        value_wide[high, :] = jnp.zeros((WINDOW, 128), jnp.bfloat16)
+
+    for r in range(edge):
+        for g in (r, edge + tokens // GRID_W + r):
+            at = pl.ds(g * GRID_W, GRID_W)
+            twice(turn(key_wide[at, :], g), key_twice, at)
+            twice(value_wide[at, :], value_twice, at)
+
+    reach = half + 2 * WINDOW
+    gap = lax.broadcasted_iota(jnp.int32, (half, reach), 1) - lax.broadcasted_iota(
+        jnp.int32, (half, reach), 0
+    )
+    spot = lax.broadcasted_iota(jnp.int32, (half, reach), 1)
+    groups = query.shape[1] // keys.shape[1]
+
+    def attend(first):
+        place = spot + (me * tokens + first - WINDOW)
+        kept = (gap >= 0) & (gap <= 2 * WINDOW) & (place >= 0) & (place < count * tokens)
+        both = jnp.concatenate([kept, kept], axis=0)
+        near = pl.ds(first, reach)
+        top = lax.broadcasted_iota(jnp.int32, (2 * half, 1), 0) < half
+        for j in range(query.shape[1] // 128):
+            head = 2 * j // groups
+            q = turned[pl.ds(first, half), pl.ds(j * 128, 128)]
+            none = jnp.zeros_like(q)
+            q = jnp.concatenate([jnp.where(left, q, none), jnp.where(left, none, q)], axis=0)
+            scores = lax.dot_general(
+                q, key_twice[head, near, :], (((1,), (1,)), ((), ())),
+                preferred_element_type=jnp.float32,
+            )
+            scores = jnp.where(both, scores, -jnp.inf)
+            sink = jnp.where(top, sinks[2 * j], sinks[2 * j + 1])
+            largest = jnp.maximum(jnp.max(scores, axis=-1, keepdims=True), sink)
+            grown = jnp.exp(scores - largest)
+            below = jnp.sum(grown, axis=-1, keepdims=True) + jnp.exp(sink - largest)
+            probs = (grown * (1.0 / below)).astype(jnp.bfloat16)
+            mixed = jnp.dot(probs, value_twice[head, near, :], preferred_element_type=jnp.float32)
+            attended[:, pl.ds(j * 128, 128)] = jnp.where(
+                left, mixed[:half], mixed[half:]
+            ).astype(jnp.bfloat16)
+        partial[pl.ds(first, half), :] = jnp.dot(
+            attended[...], w_out[...], preferred_element_type=jnp.float32
+        ).astype(jnp.bfloat16)
 
     def to_mate(i):
         return send(
@@ -175,8 +251,12 @@
         scale = lax.rsqrt(jnp.mean(x * x, axis=-1, keepdims=True) + NORM_EPS)
         normed[at, :] = (x * scale * gain[...]).astype(jnp.bfloat16)
 
+    loads[0].wait()
+    attend(theirs)
     for i in range(pieces):
         to_mate(i).start()
+    attend(mine)
+    loads[1].wait()
     for i in range(pieces):
         to_mate(i).wait_recv()
         at = pl.ds(i * rows, rows)
@@ -185,6 +265,31 @@
             + from_mate[at, :].astype(jnp.float32)
         ).astype(jnp.bfloat16)
         to_across(i).start()
+    quarter = own.shape[1]
+    lanes = -(-count // 128) * 128
+    expert_ids = lax.broadcasted_iota(jnp.int32, (tokens, lanes), 1)
+    names = [routes[:, k : k + 1] == expert_ids for k in range(2)]
+    counted = jnp.where(names[0] | names[1], 1.0, 0.0).astype(jnp.bfloat16)
+    older = lax.broadcasted_iota(jnp.int32, (tokens, tokens), 1) < lax.broadcasted_iota(
+        jnp.int32, (tokens, tokens), 0
+    )
+    before = jnp.dot(
+        jnp.where(older, 1.0, 0.0).astype(jnp.bfloat16), counted,
+        preferred_element_type=jnp.float32,
+    )
+    slot_ids = lax.broadcasted_iota(jnp.int32, (tokens, count * quarter), 1)
+    slot_ids = slot_ids.astype(jnp.float32)
+    begin = (here * quarter).astype(jnp.float32)
+    chosen = jnp.zeros((tokens, count * quarter), jnp.float32)
+    for k in range(2):
+        slot = jnp.sum(jnp.where(names[k], before, 0.0), axis=1, keepdims=True)
+        expert = routes[:, k : k + 1].astype(jnp.float32)
+        target[:, k : k + 1] = expert * (4 * quarter) + slot
+        inside = slot - begin
+        fits = (inside >= 0.0) & (inside < quarter)
+        row = jnp.where(fits, expert * quarter + inside, -1.0)
+        chosen = jnp.where(slot_ids == row, 1.0, chosen)
+    chosen = chosen.astype(jnp.bfloat16)
     for i in range(pieces):
         to_across(i).wait_recv()
         at = pl.ds(i * rows, rows)
@@ -200,11 +305,9 @@
         normalise(pl.ds(theirs + i * rows, rows))
     width = stream_cols.shape[1]
     stream_cols[...] = stream[:, pl.ds(pl.multiple_of(here * width, 128), width)]
-    quarter = own.shape[1]
-    rowid = lax.broadcasted_iota(jnp.int32, (count * quarter, places.shape[1]), 0)
-    chosen = (rowid == places[0:1, :]) | (rowid == places[1:2, :])
-    chosen = jnp.where(chosen, 1.0, 0.0).astype(jnp.bfloat16)
-    picked = jnp.dot(chosen, normed[...], preferred_element_type=jnp.float32).astype(jnp.bfloat16)
+    picked = lax.dot_general(
+        chosen, normed[...], (((0,), (0,)), ((), ())), preferred_element_type=jnp.float32
+    ).astype(jnp.bfloat16)
     for e in range(count):
         own[e] = picked[e * quarter : (e + 1) * quarter, :]
 
@@ -247,22 +350,47 @@
     def landed(k):
         return gathered.at[source(k), here]
 
-    def pass_on(j, last):
+    def expert_rows(k):
+        parts = [gathered[source(k), q] for q in range(4)]
+        if quarter % 16:
+            parts = [part.astype(jnp.float32) for part in parts]
+        rows_in = jnp.concatenate(parts, axis=0).astype(jnp.bfloat16)
+        gate = jnp.dot(rows_in, w_gate[...], preferred_element_type=jnp.float32)
+        raised = jnp.dot(rows_in, w_up[...], preferred_element_type=jnp.float32)
+        hidden[source(k)] = (jax.nn.silu(gate) * raised).astype(jnp.bfloat16)
+
+    def settle(k):
+        to_near(k, landed(k)).wait_recv()
+        to_relay(k).wait_recv()
+        expert_rows(k)
+
+    def pass_on(j, carry):
+        last, older = carry
         k = shift_at(j, count)
         to_expert(k).wait_recv()
         to_side(k, landed(k)).start()
         to_near(k, landed(k)).start()
         to_side(last, landed(last)).wait_recv()
         to_relay(last).start()
-        return k
-
-    last = lax.fori_loop(0, count - 1, pass_on, 0)
+
+        @pl.when(j > 0)
+        def _():
+            settle(older)
+
+        return k, last
+
+    for load in loads[2:]:
+        load.wait()
+    kept.wait()
+    last, older = lax.fori_loop(0, count - 1, pass_on, (0, 0))
+    settle(older)
     to_side(last, landed(last)).wait_recv()
     to_relay(last).start()
+    settle(last)
 
     def finish(k, carry):
-        to_near(k, landed(k)).wait()
-        to_relay(k).wait()
+        to_near(k, landed(k)).wait_send()
+        to_relay(k).wait_send()
         to_side(k, landed(k)).wait_send()
         return carry
 
@@ -273,27 +401,54 @@
         return carry
 
     lax.fori_loop(1, count, finish_slot, 0)
-    kept.wait()
     for i in range(pieces):
         to_mate(i).wait_send()
         to_across(i).wait_send()
         to_back(i, mine).wait_send()
 
-
-def project_dispatch(partial, residual, gain, places, count, quarter, cols, pieces):
-    rows, width = partial.shape
+    @pl.when(me < count - 1)
+    def _():
+        halo(0, True).wait_send()
+        halo(1, True).wait_send()
+
+    @pl.when(me > 0)
+    def _():
+        halo(0, False).wait_send()
+        halo(1, False).wait_send()
+
+
+def project_dispatch(operands, count, quarter, cols, pieces):
+    query, keys = operands[1], operands[2]
+    w_out, residual, w_gate, w_up = operands[-4:]
+    rows, width = residual.shape
     half = rows // 2
+    wide = (rows + 2 * WINDOW, keys.shape[1])
     dma = pltpu.SemaphoreType.DMA
     bf = jnp.bfloat16
     return pl.pallas_call(
         lambda *refs: project_dispatch_kernel(count, pieces, *refs),
         out_shape=(
-            jax.ShapeDtypeStruct((count, 4, quarter, width), bf),
+            jax.ShapeDtypeStruct((count, 4 * quarter, w_up.shape[1]), bf),
             jax.ShapeDtypeStruct((rows, cols), bf),
+            jax.ShapeDtypeStruct((rows, 2), jnp.float32),
         ),
-        in_specs=[VMEM] * 4,
-        out_specs=(VMEM, VMEM),
+        in_specs=[pl.BlockSpec(memory_space=pltpu.SMEM)]
+        + [VMEM] * 8
+        + [pl.BlockSpec(memory_space=pl.ANY)] * 4,
+        out_specs=(VMEM, VMEM, VMEM),
         scratch_shapes=[
+            pltpu.VMEM((count, 4, quarter, width), bf),
+            pltpu.VMEM(w_gate.shape, bf),
+            pltpu.VMEM(w_up.shape, bf),
+            pltpu.VMEM(wide, bf),
+            pltpu.VMEM(wide, bf),
+            pltpu.VMEM((2, *wide), bf),
+            pltpu.VMEM((2, *wide), bf),
+            pltpu.VMEM(query.shape, bf),
+            pltpu.VMEM((half, query.shape[1]), bf),
+            pltpu.VMEM(w_out.shape, bf),
+            pltpu.VMEM((rows, width), bf),
+            pltpu.VMEM((rows, width), bf),
             pltpu.VMEM((half, width), bf),
             pltpu.VMEM((half, width), bf),
             pltpu.VMEM((half, width), bf),
@@ -308,20 +463,24 @@
             dma((2, count)),
             dma((2, count)),
             dma,
+            dma((2, 2, 2)),
+            dma((4,)),
         ],
         compiler_params=pltpu.CompilerParams(
             collective_id=0, has_side_effects=True, vmem_limit_bytes=VMEM_LIMIT
         ),
-    )(partial, residual, gain, places)
+    )(*operands)
 
 
 def combine_kernel(
     count,
-    partial,
+    hidden,
+    w_down,
     stream_cols,
     target,
     weight,
     out,
+    partial,
     from_mate,
     pair,
     from_across,
@@ -367,11 +526,12 @@
         )
 
     def start_mate(j, carry):
+        partial[dest(order(j))] = jnp.dot(
+            hidden[dest(order(j))], w_down[...], preferred_element_type=jnp.float32
+        ).astype(jnp.bfloat16)
         to_mate(order(j), 1).start()
         to_mate(order(j), 0).start()
         return carry
-
-    lax.fori_loop(0, count, start_mate, 0)
 
     def start_across(j, carry):
         k = order(j)
@@ -383,7 +543,13 @@
         to_across(k).start()
         return carry
 
-    lax.fori_loop(0, count, start_across, 0)
+    def lead(j, carry):
+        start_mate(j + 1, carry)
+        return start_across(j, carry)
+
+    start_mate(0, 0)
+    lax.fori_loop(0, count - 1, lead, 0)
+    start_across(count - 1, 0)
 
     def start_back(j, carry):
         k = order(j)
@@ -406,9 +572,10 @@
     kept.start()
     mix[...] = jnp.zeros_like(mix)
     slot_ids = lax.broadcasted_iota(jnp.int32, (out.shape[0], slots), 1)
+    slot_ids = slot_ids.astype(jnp.float32)
 
     def add(expert):
-        ids = slot_ids + expert * slots
+        ids = slot_ids + (expert * slots).astype(jnp.float32)
         table = jnp.where(ids == target[:, 0:1], weight[:, 0:1], 0.0) + jnp.where(
             ids == target[:, 1:2], weight[:, 1:2], 0.0
         )
@@ -446,17 +613,18 @@
     lax.fori_loop(1, count, finish_back, 0)
 
 
-def combine(partial, stream_cols, target, weight):
-    count, slots, _ = partial.shape
+def combine(hidden, w_down, stream_cols, target, weight):
+    count, slots, _ = hidden.shape
     cols = stream_cols.shape[1]
     dma = pltpu.SemaphoreType.DMA
     bf = jnp.bfloat16
     return pl.pallas_call(
         lambda *refs: combine_kernel(count, *refs),
         out_shape=jax.ShapeDtypeStruct(stream_cols.shape, bf),
-        in_specs=[VMEM] * 4,
+        in_specs=[VMEM] * 5,
         out_specs=VMEM,
         scratch_shapes=[
+            pltpu.VMEM((count, slots, w_down.shape[1]), bf),
             pltpu.VMEM((count, 2, slots, cols), bf),
             pltpu.VMEM((count, slots, cols), bf),
             pltpu.VMEM((count, slots, cols), bf),
@@ -471,7 +639,7 @@
         compiler_params=pltpu.CompilerParams(
             collective_id=1, has_side_effects=True, vmem_limit_bytes=VMEM_LIMIT
         ),
-    )(partial, stream_cols, target, weight)
+    )(hidden, w_down, stream_cols, target, weight)
 
 
 def local(
@@ -488,55 +656,37 @@
     w_up,
     w_down,
 ):
-    tok_rows = query_proj.shape[0]
+    tok_rows, _ = query_proj.shape
+    width = residual.shape[1]
     seq_devices = lax.axis_size("sp")
-    total_rows = tok_rows * seq_devices
-    offset = lax.axis_index("sp") * tok_rows
-    kv_width = key_projection.shape[1]
-    joined = jnp.concatenate([key_projection, value_projection], axis=1)
-    widened = padded(joined, (("sp", 0),), WINDOW)
-    query_pos = offset + jnp.arange(tok_rows, dtype=jnp.int32)
-    key_pos = offset - WINDOW + jnp.arange(tok_rows + 2 * WINDOW, dtype=jnp.int32)
-    rot_q = axial_rotation(query_proj.reshape(tok_rows, -1, HEAD_SIZE), query_pos).astype(
-        jnp.bfloat16
-    )
-    rotated_keys = axial_rotation(
-        widened[:, :kv_width].reshape(-1, kv_width // HEAD_SIZE, HEAD_SIZE), key_pos
-    ).astype(jnp.bfloat16)
-    value_head_rows = widened[:, kv_width:].reshape(-1, kv_width // HEAD_SIZE, HEAD_SIZE)
-    attended = attend_block(
-        rot_q, rotated_keys, value_head_rows, sink_logit, query_pos, key_pos, total_rows
-    )
-    partial_value = jnp.dot(attended, w_out, preferred_element_type=jnp.float32)
-    width = partial_value.shape[1]
     col_blocks = lax.axis_size("tp")
     col_width = width // col_blocks
-    top_count = routes.shape[1]
     experts = w_gate.shape[0] * seq_devices
-    capacity = 2 * top_count * tok_rows // experts
+    capacity = 2 * routes.shape[1] * tok_rows // experts
     quarter = capacity // col_blocks
-    expert_ids = jnp.arange(experts, dtype=jnp.int32)
-    named = routes[:, :, None] == expert_ids
-    counted = jnp.any(named, axis=1).astype(jnp.bfloat16)
-    earlier = jnp.tri(tok_rows, k=-1, dtype=jnp.bfloat16)
-    before = jnp.dot(earlier, counted, preferred_element_type=jnp.float32)
-    slot_number = jnp.sum(jnp.where(named, before[:, None, :], 0.0), axis=2).astype(jnp.int32)
-    destination = routes * capacity + slot_number
-    inside = slot_number - lax.axis_index("tp") * quarter
-    places = jnp.where((inside >= 0) & (inside < quarter), routes * quarter + inside, -1).T
-    gathered, stream_cols = project_dispatch(
-        partial_value.astype(jnp.bfloat16), residual, norm_gain[None, :], places,
+    half_dim = HEAD_SIZE // 2
+    inverse = ROPE_BASE ** (-jnp.arange(0, half_dim, 2, dtype=jnp.float32) / half_dim)
+    lane_rates = jnp.tile(inverse, 128 // inverse.shape[0])
+    lane = jnp.arange(128)
+    first = lane % half_dim < half_dim // 2
+    partner = jnp.where(first, lane + half_dim // 2, lane - half_dim // 2)
+    swap = jnp.where(
+        lane[:, None] == partner[None, :], jnp.where(first, -1.0, 1.0)[None, :], 0.0
+    ).astype(jnp.bfloat16)
+    grid_rows = (tok_rows + 2 * WINDOW) // GRID_W
+    first_row = lax.axis_index("sp") * (tok_rows // GRID_W) - WINDOW // GRID_W
+    row_angles = (first_row + jnp.arange(grid_rows)).astype(jnp.float32)[:, None] * lane_rates
+    col_angles = jnp.arange(GRID_W, dtype=jnp.float32)[:, None] * lane_rates
+    row_turn = jnp.stack([jnp.cos(row_angles), jnp.sin(row_angles)])
+    col_turn = jnp.stack([jnp.cos(col_angles), jnp.sin(col_angles)])
+    hidden, stream_cols, destination = project_dispatch(
+        (
+            sink_logit, query_proj, key_projection, value_projection, row_turn, col_turn, swap,
+            norm_gain[None, :], routes, w_out, residual, w_gate[0], w_up[0],
+        ),
         seq_devices, quarter, col_width, 4,
     )
-    expert_rows = gathered.reshape(-1, width)
-    gate_part = jnp.dot(expert_rows, w_gate[0], preferred_element_type=jnp.float32)
-    up_part = jnp.dot(expert_rows, w_up[0], preferred_element_type=jnp.float32)
-    hidden = (jax.nn.silu(gate_part) * up_part).astype(jnp.bfloat16)
-    partial_rows = jnp.dot(hidden, w_down[0], preferred_element_type=jnp.float32)
-    return combine(
-        partial_rows.astype(jnp.bfloat16).reshape(seq_devices, capacity, width),
-        stream_cols, destination, route_weights,
-    )
+    return combine(hidden, w_down[0], stream_cols, destination, route_weights)
 
 
 def solution(mesh):

time: 162 us -> 120 us (0.74)
  matrix products: 27.1 us -> 0 us
  other arithmetic: 12.5 us -> 2.14 us
  Pallas kernels: 104 us -> 113 us
  starting transfers between devices: 6.8 us -> 0 us
  local copies, waits for them, and re-layouts: 10.4 us -> 4.69 us
    dot_general x6 -> x0, matrix products: 27.1 us -> none  [the longest x1 12.1 us: local(): jnp.dot(hidden, w_down[0], preferred_element_type=jnp.float32)]
    pallas_call x1, Pallas kernels: 57.7 us -> 66.3 us  [project_dispatch(): pl.pallas_call(lambda *refs: project_dispatch_kernel(count, pieces, *refs...]
    ppermute x2 -> x0, starting transfers between devices: 6.8 us -> none  [the longest x1 5.52 us: padded(): lax.ppermute(tail, axis, [(i, (i + 1) % count) for i in range(ends)])]
    unnamed x12 -> x3, local copies, waits for them, and re-layouts: 7.1 us -> 4.61 us
    cos x2, other arithmetic: 2.42 us -> 0.25 us  [the longest x1 0.14 us: local(): col_turn = jnp.stack([jnp.cos(col_angles), jnp.sin(col_angles)])]
    add x4 -> x0, other arithmetic: 1.94 us -> none  [the longest x1 1.28 us: local(): destination = routes * capacity + slot_number]
  transfers between devices with their start and end apart: 2 -> 0, of which waited for: 0 -> 0; matrix products, arithmetic and copies ran while one was open for 9% -> 0% of each run, Pallas kernels for 0% -> 0%
where the time goes in v2:
time: 120 us
  Pallas kernels  113 us (94%)
  local copies, waits for them, and re-layouts  4.69 us (4%)
  other arithmetic  2.14 us (2%)
    pallas_call x1, Pallas kernels, project_dispatch(): pl.pallas_call(lambda *refs: project_dispatch_kernel(count, pieces, *refs...  66.3 us
    pallas_call x1, Pallas kernels, combine(): pl.pallas_call(lambda *refs: combine_kernel(count, *refs), out_shape=jax....  46.9 us
    unnamed x3, local copies, waits for them, and re-layouts  4.61 us

profile of v2, /device:TPU:0, one launch (start us, length us, event | category | flops | bytes accessed | tf_op | source)
XLA Modules:
  0.0 120.1 jit_solution(11833361535832869704)
XLA Ops:
  0.0 0.1 mul.77
  0.1 0.1 multiply_cosine_fusion
  0.2 0.6 pad_maximum_fusion.1.refs_4_
  0.8 0.6 select_convert_fusion.refs_6_
  1.5 0.1 fusion.1
  1.6 0.6 pad_maximum_fusion.refs_5_
  2.2 1.5 %copy.13.refs_8_ = s32[256,2]{1,0:T(8,128)} copy(s32[256,2]{0,1:T(2,128)} %param.19) | data formatting | bytes 4096 | tf_op args[7]
  3.7 1.5 %copy.14.refs_4_ = f32[256,2]{1,0:T(8,128)} copy(f32[256,2]{0,1:T(2,128)} %param.20) | data formatting | bytes 4096 | tf_op args[8]
  5.2 66.3 %shard_map.118 = (bf16[8,128,640]{2,1,0:T(8,128)(2,1)}, bf16[256,512]{1,0:T(8,128)(2,1)}, f32[256,2]{1,0:T(8,128)}) custom-call(f32[8]{0:T(128)} %refs_0_.1, bf16[256,512]{1,0:T(8,128)(2,1)} %refs_1_.1, bf16[256,128]{1,0:T(8,128)(2,1)} %refs_2_.1, bf16[256,128]{1,0:T(8,128)(2,1)} %refs_3_.1, f32[2,8,128]{2,1,0:T(8,128)} %pad_maximum_fusion.1.refs_4_, ...), custom_call_target="tpu_custom_call" | custom-call | tf_op jit(solution)/shard_map/pallas_call | solution.py:428
  71.5 46.9 %shard_map.119 = bf16[256,512]{1,0:T(8,128)(2,1)} custom-call(bf16[8,128,640]{2,1,0:T(8,128)(2,1)} %get-tuple-element.8.refs_0_, bf16[640,2048]{1,0:T(8,128)(2,1)} %bitcast.4, bf16[256,512]{1,0:T(8,128)(2,1)} %get-tuple-element.9.refs_2_, f32[256,2]{1,0:T(8,128)} %get-tuple-element.10.refs_3_, f32[256,2]{1,0:T(8,128)} %copy.14.refs_4_), custom_call_target="tpu_custom_call" | custom-call | tf_op jit(solution)/shard_map/pallas_call | solution.py:621
  118.4 1.7 %copy.16 = bf16[256,512]{1,0:T(8,128)(2,1)} copy(bf16[256,512]{1,0:T(8,128)(2,1)} %shard_map.119) | data formatting | bytes 524288
  (5 shorter events, 0.0 us)
